TPU v7x, 32 devices: a whole 2x2x4 slice. The times are simulated.
32 devices in a mesh: ep: 16 (over z, y, x), tp: 2 (over core).
Axes of the slice: x: 2, y: 2, z: 4, core: 2. Of those that a mesh axis runs over, the one named last changes fastest.
Arguments:
- resid: bfloat16 [256, 2048], P('ep'), may hold values from -6 to 6
- proj_x: bfloat16 [256, 2048], P('ep', 'tp'), may hold values from -6 to 6
- proj_z: bfloat16 [256, 2048], P('ep', 'tp'), may hold values from -6 to 6
- proj_bc: bfloat16 [256, 2, 512], P('ep', None, 'tp'), may hold values from -6 to 6
- proj_dt: bfloat16 [256, 32], P('ep', 'tp'), may hold values from -6 to 6
- tail_x: bfloat16 [256, 3, 2048], P('ep', None, 'tp'), may hold values from -6 to 6
- tail_bc: bfloat16 [256, 3, 2, 512], P('ep', None, None, 'tp'), may hold values from -6 to 6
- taps_x: bfloat16 [4, 2048], P(None, 'tp'), may hold values from -3 to 3
- taps_bc: bfloat16 [4, 2, 512], P(None, None, 'tp'), may hold values from -3 to 3
- ssm_state: float32 [256, 32, 4096], P('ep', 'tp'), may hold values from -1.5 to 1.5
- dt_bias: float32 [32], P('tp'), may hold values from -4 to 0
- decay_log: float32 [32], P('tp'), may hold values from -1 to 2.5
- group_gain: float32 [2048], P('tp'), may hold values from 0.1 to 1.9
- out_proj: bfloat16 [2048, 2048], P('tp', 'ep'), may hold values from -0.125 to 0.125
- ffn_gain: float32 [2048], replicated, may hold values from 0.1 to 1.9
- dense_gate: bfloat16 [2048, 4096], P(None, ('ep', 'tp')), may hold values from -0.125 to 0.125
- dense_up: bfloat16 [2048, 4096], P(None, ('ep', 'tp')), may hold values from -0.125 to 0.125
- dense_down: bfloat16 [4096, 2048], P(('ep', 'tp')), may hold values from -0.09375 to 0.09375
- branch_gate: bfloat16 [2048], replicated, may hold values from -0.125 to 0.125
- group_weights: float32 [256, 4], replicated, may hold values from 0.2 to 1
- expert_ids: int32 [256, 6], replicated, may hold values from 0 to 15, all different within a row; in each aligned block of 16 rows (0 to 15, 16 to 31, ...) at most 7 rows name the same one
- expert_weights: float32 [256, 6], replicated, may hold values from 0.1 to 1
- exp_gate: bfloat16 [16, 2048, 512], P('ep', None, 'tp'), may hold values from -0.125 to 0.125
- exp_up: bfloat16 [16, 2048, 512], P('ep', None, 'tp'), may hold values from -0.125 to 0.125
- exp_down: bfloat16 [16, 512, 2048], P('ep', 'tp'), may hold values from -0.25 to 0.25
Outputs:
- out: bfloat16 [256, 2048], P(('ep', 'tp'))
- new_state: float32 [256, 32, 4096], P('ep', 'tp')
Inputs may be any that keep to these rules, and one draw needn't show every extreme that they name: `expert_ids`: each row names 6 different experts. In the rows of one index of ep (aligned blocks of 16 rows) no expert is named more than 7 times, a bound that some block reaches.
All inputs are finite; a program needn't handle non-finite values.
Results may differ from a plain program's by a relative error of at most 0.013.
Values may be sent and summed in bfloat16 or wider, within the bound.
A program may use at most 128 MiB of HBM per device.

v0:
```python
import jax
import jax.numpy as jnp
from jax import lax
from jax.sharding import PartitionSpec as P

HEAD_P = 64
NSTATE = 64
GROUPS = 4
TOPK = 6
HPG = 4


EPSILON = 1e-06


def state_update(
    proj_x,
    proj_z,
    proj_bc,
    proj_dt,
    tail_x,
    tail_bc,
    taps_x,
    taps_bc,
    ssm_state,
    dt_bias,
    decay_log,
    group_gain,
):
    window_x = jnp.concatenate([tail_x, proj_x[:, None]], axis=1).astype(jnp.float32)
    conv_x = jax.nn.silu(jnp.sum(window_x * taps_x.astype(jnp.float32)[None], axis=1))
    window_bc = jnp.concatenate([tail_bc, proj_bc[:, None]], axis=1).astype(jnp.float32)
    conv_bc = jax.nn.silu(jnp.sum(window_bc * taps_bc.astype(jnp.float32)[None], axis=1))
    count = proj_x.shape[0]
    heads = proj_dt.shape[1]
    x_heads = conv_x.reshape(count, heads, HEAD_P)
    grouped_bc = conv_bc.reshape(count, 2, heads // HPG, NSTATE)
    input_heads = jnp.repeat(grouped_bc[:, 0], HPG, axis=1)
    read_heads = jnp.repeat(grouped_bc[:, 1], HPG, axis=1)
    step_size = jax.nn.softplus(proj_dt.astype(jnp.float32) + dt_bias)
    decay = jnp.exp(-step_size * jnp.exp(decay_log))
    state = ssm_state.reshape(count, heads, HEAD_P, NSTATE)
    fresh = (step_size[:, :, None] * x_heads)[:, :, :, None] * input_heads[:, :, None, :]
    new_state = decay[:, :, None, None] * state + fresh
    readout = jnp.sum(new_state * read_heads[:, :, None, :], axis=-1)
    gated = readout.reshape(count, heads * HEAD_P) * jax.nn.silu(proj_z.astype(jnp.float32))
    grouped = gated.reshape(count, heads // HPG, HPG * HEAD_P)
    grouped = grouped * lax.rsqrt(jnp.mean(grouped * grouped, axis=-1, keepdims=True) + EPSILON)
    y_out = (grouped.reshape(count, heads * HEAD_P) * group_gain).astype(jnp.bfloat16)
    return (y_out, new_state.reshape(count, heads, HEAD_P * NSTATE))


def shards(
    resid,
    proj_x,
    proj_z,
    proj_bc,
    proj_dt,
    tail_x,
    tail_bc,
    taps_x,
    taps_bc,
    ssm_state,
    dt_bias,
    decay_log,
    group_gain,
    out_proj,
    ffn_gain,
    dense_gate,
    dense_up,
    dense_down,
    branch_gate,
    group_weights,
    expert_ids,
    expert_weights,
    exp_gate,
    exp_up,
    exp_down,
):
    y_out, new_state = state_update(
        proj_x,
        proj_z,
        proj_bc,
        proj_dt,
        tail_x,
        tail_bc,
        taps_x,
        taps_bc,
        ssm_state,
        dt_bias,
        decay_log,
        group_gain,
    )
    partial_value = jnp.dot(
        lax.all_gather(y_out, "ep", axis=0, tiled=True),
        out_proj,
        preferred_element_type=jnp.float32,
    )
    partial_value = lax.all_to_all(
        partial_value.astype(jnp.bfloat16), "ep", split_axis=0, concat_axis=1, tiled=True
    ).astype(partial_value.dtype)
    mixed = lax.psum(partial_value.astype(jnp.bfloat16), "tp").astype(jnp.float32)
    resid_new = (resid.astype(jnp.float32) + mixed).astype(jnp.bfloat16)
    widened = resid_new.astype(jnp.float32)
    normed = (
        widened
        * lax.rsqrt(jnp.mean(widened * widened, axis=-1, keepdims=True) + EPSILON)
        * ffn_gain
    ).astype(jnp.bfloat16)
    gathered = lax.all_gather(normed, "ep", axis=0, tiled=True)
    score = jnp.dot(gathered, branch_gate, preferred_element_type=jnp.float32)
    dense_pre = jnp.dot(gathered, dense_gate, preferred_element_type=jnp.float32)
    dense_lin = jnp.dot(gathered, dense_up, preferred_element_type=jnp.float32)
    dense_hidden = (jax.nn.sigmoid(score)[:, None] * jax.nn.silu(dense_pre) * dense_lin).astype(
        jnp.bfloat16
    )
    experts = lax.axis_size("ep")
    expert_own = lax.axis_index("ep")
    cores = lax.axis_size("tp")
    core_index = lax.axis_index("tp")
    batch = gathered.shape[0]
    rows_each = batch // experts
    half_rows = rows_each // cores
    pairs = rows_each * TOPK
    capacity = (pairs + experts - 1) // experts + 1
    group_size = experts // GROUPS
    levels = jnp.arange(1, capacity + 1, dtype=jnp.int32)
    pair_row = jnp.arange(pairs, dtype=jnp.int32) // TOPK
    pick = (jnp.arange(GROUPS, dtype=jnp.int32) == expert_own // group_size).astype(jnp.float32)
    coarse = jnp.sum(group_weights * pick[None], axis=1)
    pair_weight = (expert_weights * coarse[:, None]).reshape(experts, pairs)
    hits = (expert_ids.reshape(experts, pairs) == expert_own).astype(jnp.int32)
    ranks = jnp.cumsum(hits, axis=1, dtype=jnp.int32)
    select = hits[:, None, :] * (ranks[:, None, :] == levels[None, :, None]).astype(jnp.int32)
    local_row = jnp.sum(select * pair_row[None, None, :], axis=-1, dtype=jnp.int32)
    filled = jnp.sum(select, axis=-1, dtype=jnp.int32).reshape(-1)
    slot_weight = jnp.sum(select.astype(jnp.float32) * pair_weight[:, None, :], axis=-1).reshape(-1)
    row_index = (local_row + jnp.arange(experts, dtype=jnp.int32)[:, None] * rows_each).reshape(-1)
    slot_rows = jnp.take(gathered, row_index, axis=0)
    slot_pre = jnp.dot(slot_rows, exp_gate[0], preferred_element_type=jnp.float32)
    slot_lin = jnp.dot(slot_rows, exp_up[0], preferred_element_type=jnp.float32)
    slot_hidden = (slot_weight[:, None] * jax.nn.silu(slot_pre) * slot_lin).astype(jnp.bfloat16)
    placing = (jnp.arange(batch, dtype=jnp.int32)[:, None] == row_index[None, :]) & (
        filled[None, :] > 0
    )
    row_hidden = jnp.dot(
        placing.astype(jnp.bfloat16), slot_hidden, preferred_element_type=jnp.float32
    ).astype(jnp.bfloat16)
    joined = jnp.concatenate([dense_hidden, row_hidden], axis=1)
    down_all = jnp.concatenate([dense_down, exp_down[0]], axis=0)
    inner_width = joined.shape[1]
    ordered = (
        joined.reshape(experts, cores, half_rows, inner_width)
        .transpose(1, 0, 2, 3)
        .reshape(batch, inner_width)
    )
    halved = lax.psum_scatter(
        jnp.dot(ordered, down_all, preferred_element_type=jnp.float32).astype(jnp.bfloat16),
        "tp",
        scatter_dimension=0,
        tiled=True,
    ).astype(jnp.float32)
    branch = lax.psum_scatter(halved, "ep", scatter_dimension=0, tiled=True)
    own_rows = lax.dynamic_slice_in_dim(widened, core_index * half_rows, half_rows, 0)
    out = (own_rows + branch).astype(jnp.bfloat16)
    return (out, new_state)


def solution(mesh):
    return jax.shard_map(
        shards,
        mesh=mesh,
        in_specs=(
            P("ep", None),
            P("ep", "tp"),
            P("ep", "tp"),
            P("ep", None, "tp"),
            P("ep", "tp"),
            P("ep", None, "tp"),
            P("ep", None, None, "tp"),
            P(None, "tp"),
            P(None, None, "tp"),
            P("ep", "tp", None),
            P("tp"),
            P("tp"),
            P("tp"),
            P("tp", "ep"),
            P(),
            P(None, ("ep", "tp")),
            P(None, ("ep", "tp")),
            P(("ep", "tp"), None),
            P(),
            P(),
            P(),
            P(),
            P("ep", None, "tp"),
            P("ep", None, "tp"),
            P("ep", "tp", None),
        ),
        out_specs=(P(("ep", "tp"), None), P("ep", "tp", None)),
        check_vma=False,
    )
```

profile of v0, /device:TPU:0, one launch (start us, length us, event | category | flops | bytes accessed | tf_op | source)
XLA Modules:
  0.0 270.5 jit_solution(9776574114942145212)
XLA Ops:
  7.2 0.7 exp.39
  7.9 0.7 convert_element_type.90
  8.6 0.9 multiply_reduce_fusion.3
  9.6 0.1 reduce_sum.88
  9.7 0.7 convert_element_type.88
  10.4 0.9 multiply_reduce_fusion.1
  11.4 0.1 reduce_sum.86
  11.5 7.9 %reshape.179 = f32[16,16,64,64]{3,2,1,0:T(8,128)} reshape(f32[16,16,4096]{2,1,0:T(8,128)} %param.34) | data formatting | bytes 8388608 | tf_op jit(solution)/shard_map/reshape | solution.py:42
  19.4 0.1 multiply_multiply_fusion
  19.7 8.5 %broadcast_multiply_fusion = (f32[16,16,64,64]{3,2,1,0:T(8,128)}, f32[16,16,64]{2,1,0:T(8,128)S(1)}) fusion(f32[16,16,64]{2,1,0:T(8,128)S(1)} %bitcast.44, f32[16,16,64]{2,1,0:T(8,128)S(1)} %multiply_multiply_fusion, f32[16,16,64]{2,1,0:T(8,128)S(1)} %bitcast.45, f32[16,16,64,64]{3,2,1,0:T(8,128)} %reshape.179, f32[16,16]{1,0:T(8,128)S(1)} %get-tuple-element.11), kind=kLoop, calls=%fused_computation.3 | loop fusion | flops 5226496 | bytes 8651776 | tf_op jit(solution)/shard_map/mul | solution.py:43
  28.2 0.1 reshape.180
  28.4 0.1 reduce_sum.90
  28.7 45.3 %all_gather.6 = bf16[256,1024]{1,0:T(8,128)(2,1)S(1)} all-gather(bf16[16,1024]{1,0:T(8,128)(2,1)S(1)} %multiply_convert_fusion.1), channel_id=1, replica_groups=mesh['ep'=16,'tp'=2] {'ep'}, dimensions={0}, use_global_device_ids=true | all-gather | bytes 557056 | tf_op jit(solution)/shard_map/all_gather | solution.py:95
  74.0 0.9 convolution_convert_fusion.2
  74.9 3.5 %all-to-all-start = ((bf16[16,16,128]{2,1,0:T(8,128)(2,1)}), bf16[16,16,128]{2,1,0:T(8,128)(2,1)S(1)}, u32[]{:S(2)}, u32[]{:S(2)}) async-start(bf16[16,16,128]{2,1,0:T(8,128)(2,1)} %bitcast.6), calls=%async_computation | async-start | bytes 131072 | tf_op jit(solution)/shard_map/all_to_all | solution.py:99
  78.5 7.4 %all-to-all-done = bf16[16,16,128]{2,1,0:T(8,128)(2,1)S(1)} async-done(((bf16[16,16,128]{2,1,0:T(8,128)(2,1)}), bf16[16,16,128]{2,1,0:T(8,128)(2,1)S(1)}, u32[]{:S(2)}, u32[]{:S(2)}) %all-to-all-start) | async-done | bytes 65568 | tf_op jit(solution)/shard_map/all_to_all | solution.py:99
  85.9 0.6 copy_bitcast_fusion
  86.7 14.5 %all-reduce.2.cloned.1.call-done = bf16[16,2048]{1,0:T(8,128)(2,1)} async-done(((bf16[16,2048]{1,0:T(8,128)(2,1)}), bf16[16,2048]{1,0:T(8,128)(2,1)}) %all-reduce.2.cloned.1.call-update) | async-done | bytes 65552 | tf_op jit(solution)/shard_map/psum | solution.py:102
  101.2 1.0 fusion.21
  102.1 1.6 multiply_convert_fusion
  103.8 0.1 copy.39
  103.9 0.1 reshape.183
  104.0 0.3 reduce_window_sum.11
  104.3 0.4 select_reduce_fusion
  104.8 0.1 add.162
  104.9 0.1 add.159
  105.0 0.1 multiply_reduce_fusion.4
  105.1 0.1 copy.42
  105.2 0.1 mul.274
  105.4 0.2 fusion.26
  105.6 0.1 mul.277
  105.7 0.1 copy.41
  105.8 0.1 gt.18
  106.0 54.8 %all-gather.2.cloned.1.call-done = bf16[256,2048]{1,0:T(8,128)(2,1)} async-done(((bf16[16,2048]{1,0:T(8,128)(2,1)}), bf16[256,2048]{1,0:T(8,128)(2,1)}) %all-gather.2.cloned.1.call-update) | async-done | bytes 1048592 | tf_op jit(solution)/shard_map/all_gather | solution.py:110
  160.8 1.6 fusion.36
  162.4 2.8 %gather_fusion = bf16[112,2048]{1,0:T(8,128)(2,1)S(1)} fusion(bf16[256,2048]{1,0:T(8,128)(2,1)} %all-gather.2.cloned.1.call-done, s32[1024]{0:T(1024)S(1)} %pad_clamp_fusion), kind=kCustom, calls=%fused_computation | custom fusion | bytes 917952 | tf_op jit(solution)/shard_map/jit(_take)/gather | solution.py:139
  165.3 1.6 fusion.7
  166.8 0.6 convolution_convert_fusion.1
  167.5 0.5 fusion.37
  168.0 1.5 fusion.3
  169.5 0.2 copy.45
  169.7 3.0 %convolution_convert_fusion = bf16[256,2048]{1,0:T(8,128)(2,1)} fusion(bf16[256,384]{1,0:T(8,128)(2,1)S(1)} %bitcast.48, bf16[256,2048]{1,0:T(8,128)(2,1)} %bitcast.52, bf16[128,2048]{1,0:T(8,128)(2,1)} %param.42), kind=kOutput, calls=%fused_computation.4 | convolution fusion | flops 406323200 | bytes 2818048 | tf_op jit(solution)/shard_map/dot_general | solution.py:158
  172.8 7.3 %reduce-scatter.3.cloned.1.call-done = bf16[128,2048]{1,0:T(8,128)(2,1)} async-done(((bf16[256,2048]{1,0:T(8,128)(2,1)}), bf16[128,2048]{1,0:T(8,128)(2,1)}) %reduce-scatter.3.cloned.1.call-update) | async-done | bytes 524304 | tf_op jit(solution)/shard_map/reduce_scatter | solution.py:157
  180.2 2.2 convert_element_type.106
  182.4 7.9 %mul.284 = f32[16,16,4096]{2,1,0:T(8,128)} reshape(f32[16,16,64,64]{3,2,1,0:T(8,128)} %get-tuple-element.4) | data formatting | bytes 8388608 | tf_op jit(solution)/shard_map/mul | solution.py:43
  190.3 6.6 %multiply_add_fusion = f32[16,16,4096]{2,1,0:T(8,128)} fusion(f32[16,16,4096]{2,1,0:T(8,128)} %mul.284, f32[16,16,4096]{2,1,0:T(8,128)} %param.34, f32[16,16]{1,0:T(8,128)S(1)} %get-tuple-element.11), kind=kLoop, calls=%fused_computation.2 | loop fusion | flops 2097152 | bytes 12583936 | tf_op jit(solution)/shard_map/add | solution.py:44
  196.9 65.7 %reduce-scatter.5.cloned.1.call-done = f32[8,2048]{1,0:T(8,128)} async-done(((f32[128,2048]{1,0:T(8,128)}), f32[8,2048]{1,0:T(8,128)}) %reduce-scatter.5.cloned.1.call-update) | async-done | bytes 65552 | tf_op jit(solution)/shard_map/reduce_scatter | solution.py:163
  262.5 1.5 add_convert_fusion.1
  (65 shorter events, 0.9 us)
Async XLA Ops:
  7.2 159.7 %copy-start = (bf16[1,2048,256]{2,1,0:T(8,128)(2,1)S(1)}, bf16[1,2048,256]{2,1,0:T(8,128)(2,1)}, u32[]{:S(2)}) copy-start(bf16[1,2048,256]{2,1,0:T(8,128)(2,1)} %param.48) | copy-start | bytes 3145732
  11.5 7.9 %copy-start.12 = (bf16[16,16]{1,0:T(8,128)(2,1)S(1)}, bf16[16,16]{1,0:T(8,128)(2,1)}, u32[]{:S(2)}) copy-start(bf16[16,16]{1,0:T(8,128)(2,1)} %param.29) | copy-start | bytes 1540
  11.5 7.9 %copy-start.13 = (f32[16]{0:T(128)S(1)}, f32[16]{0:T(128)}, u32[]{:S(2)}) copy-start(f32[16]{0:T(128)} %param.35) | copy-start | bytes 196
  19.6 8.7 %copy-start.5 = (bf16[16,1024]{1,0:T(8,128)(2,1)S(1)}, bf16[16,1024]{1,0:T(8,128)(2,1)}, u32[]{:S(2)}) copy-start(bf16[16,1024]{1,0:T(8,128)(2,1)} %param.27) | copy-start | bytes 98308
  19.6 9.0 %copy-start.9 = (f32[1024]{0:T(1024)S(1)}, f32[1024]{0:T(1024)}, u32[]{:S(2)}) copy-start(f32[1024]{0:T(1024)} %param.37) | copy-start | bytes 12292
  19.6 54.4 %copy-start.3 = (bf16[1024,128]{1,0:T(8,128)(2,1)S(1)}, bf16[1024,128]{1,0:T(8,128)(2,1)}, u32[]{:S(2)}) copy-start(bf16[1024,128]{1,0:T(8,128)(2,1)} %param.38) | copy-start | bytes 786436
  19.6 67.0 %copy-start.7 = (s32[256,6]{0,1:T(8,128)S(1)}, s32[256,6]{0,1:T(8,128)}, u32[]{:S(2)}) copy-start(s32[256,6]{0,1:T(8,128)} %param.45) | copy-start | bytes 18436
  19.6 81.5 %copy-start.4 = (bf16[16,2048]{1,0:T(8,128)(2,1)S(1)}, bf16[16,2048]{1,0:T(8,128)(2,1)}, u32[]{:S(2)}) copy-start(bf16[16,2048]{1,0:T(8,128)(2,1)} %param.25) | copy-start | bytes 196612
  19.6 82.5 %copy-start.6 = (f32[2048]{0:T(1024)S(1)}, f32[2048]{0:T(1024)}, u32[]{:S(2)}) copy-start(f32[2048]{0:T(1024)} %param.39) | copy-start | bytes 24580
  19.7 85.3 %copy-start.11 = (f32[256,4]{0,1:T(4,128)S(1)}, f32[256,4]{0,1:T(4,128)}, u32[]{:S(2)}) copy-start(f32[256,4]{0,1:T(4,128)} %param.44) | copy-start | bytes 12292
  19.7 85.4 %copy-start.8 = (f32[256,6]{0,1:T(8,128)S(1)}, f32[256,6]{0,1:T(8,128)}, u32[]{:S(2)}) copy-start(f32[256,6]{0,1:T(8,128)} %param.46) | copy-start | bytes 18436
  19.7 86.2 %copy-start.10 = (bf16[2048]{0:T(1024)(128)(2,1)S(1)}, bf16[2048]{0:T(1024)(128)(2,1)}, u32[]{:S(2)}) copy-start(bf16[2048]{0:T(1024)(128)(2,1)} %param.43) | copy-start | bytes 12292
  74.9 11.0 %all-to-all-start = ((bf16[16,16,128]{2,1,0:T(8,128)(2,1)}), bf16[16,16,128]{2,1,0:T(8,128)(2,1)S(1)}, u32[]{:S(2)}, u32[]{:S(2)}) async-start(bf16[16,16,128]{2,1,0:T(8,128)(2,1)} %bitcast.6), calls=%async_computation | async-start | bytes 131072 | tf_op jit(solution)/shard_map/all_to_all | solution.py:99
  78.4 22.7 %all-reduce.2.cloned.1.call-start = ((), (), s32[]{:S(2)}) async-start(), calls=%async_computation.3 | async-start | bytes 131072 | tf_op jit(solution)/shard_map/psum | solution.py:102
  86.6 74.2 %all-gather.2.cloned.1.call-start = ((), (), s32[]{:S(2)}) async-start(), calls=%async_computation.4 | async-start | bytes 1114112 | tf_op jit(solution)/shard_map/all_gather | solution.py:110
  103.7 76.4 %reduce-scatter.3.cloned.1.call-start = ((), (), s32[]{:S(2)}) async-start(), calls=%async_computation.5 | async-start | bytes 1572864 | tf_op jit(solution)/shard_map/reduce_scatter | solution.py:157
  162.4 5.0 %copy-start.1 = (bf16[256,2048]{1,0:T(8,128)(2,1)S(1)}, bf16[256,2048]{1,0:T(8,128)(2,1)}, u32[]{:S(2)}) copy-start(bf16[256,2048]{1,0:T(8,128)(2,1)} %all-gather.2.cloned.1.call-done) | copy-start | bytes 3145732
  162.4 5.1 %copy-start.2 = (bf16[2048,128]{1,0:T(8,128)(2,1)S(1)}, bf16[2048,128]{1,0:T(8,128)(2,1)}, u32[]{:S(2)}) copy-start(bf16[2048,128]{1,0:T(8,128)(2,1)} %param.40) | copy-start | bytes 1572868
  172.8 89.7 %reduce-scatter.5.cloned.1.call-start = ((), (), s32[]{:S(2)}) async-start(), calls=%async_computation.6 | async-start | bytes 1114112 | tf_op jit(solution)/shard_map/reduce_scatter | solution.py:163
Sparse Core Ops, SparseCore 0:
  86.7 14.3 all-reduce.1
  104.5 56.2 all-gather.1
  172.9 7.2 reduce-scatter.2
  182.5 79.9 reduce-scatter.4
where the time goes:
time: 272 us; the launch traced here: 271 us
  waiting for transfers between devices  150 us (55%)
  blocking collectives  45.3 us (17%)
  other arithmetic  25.9 us (10%)
  local copies, waits for them, and re-layouts  21.8 us (8%)
  between operations  14.3 us (5%)
  matrix products  9.75 us (4%)
  starting transfers between devices  3.67 us (1%)
    reduce_scatter x1, waiting for transfers between devices, shards(): branch = lax.psum_scatter(halved, 'ep', scatter_dimension=0, tiled=True)  65.7 us
    all_gather x1, waiting for transfers between devices, shards(): gathered = lax.all_gather(normed, 'ep', axis=0, tiled=True)  54.8 us
    all_gather x1, blocking collectives, shards(): lax.all_gather(y_out, 'ep', axis=0, tiled=True)  45.3 us
    psum x1, waiting for transfers between devices, shards(): lax.psum(partial_value.astype(jnp.bfloat16), 'tp').astype(jnp.float32)  14.5 us
    mul x1, other arithmetic, state_update(): (step_size[:, :, None] * x_heads)[:, :, :, None]  8.51 us
    reshape x1, local copies, waits for them, and re-layouts, state_update(): state = ssm_state.reshape(count, heads, HEAD_P, NSTATE)  7.89 us
    mul x1, local copies, waits for them, and re-layouts, state_update(): (step_size[:, :, None] * x_heads)[:, :, :, None]  7.88 us
    all_to_all x1, waiting for transfers between devices, shards(): lax.all_to_all(partial_value.astype(jnp.bfloat16), 'ep', split_axis=0, co...  7.45 us
  transfers between devices with their start and end apart: 5, of which 5 were waited for; matrix products, arithmetic and copies ran while one was open for 6% of the time, Pallas kernels for 0%

commit v1 on v0

--- a/solution.py
+++ b/solution.py
@@ -1,6 +1,10 @@
+import functools
+
 import jax
 import jax.numpy as jnp
 from jax import lax
+from jax.experimental import pallas as pl
+from jax.experimental.pallas import tpu as pltpu
 from jax.sharding import PartitionSpec as P
 
 HEAD_P = 64
@@ -11,6 +15,385 @@
 
 
 EPSILON = 1e-06
+LANES = 512
+PLANE = 4
+MESH = pl.DeviceIdType.MESH
+F32 = jnp.float32
+BF16 = jnp.bfloat16
+
+
+def mm(a, b):
+    return jnp.dot(a, b, preferred_element_type=F32)
+
+
+def iota(shape, dim):
+    return lax.broadcasted_iota(jnp.int32, shape, dim)
+
+
+def one_hot(cond):
+    return cond.astype(F32).astype(BF16)
+
+
+def state_kernel(
+    x_ref, z_ref, inp_ref, rd_ref, dt_ref, bias_ref, log_ref, gain_ref, state_ref,
+    y_ref, new_ref, xs, inp_s, rd_s, decay_s, acc,
+):
+    j = pl.program_id(0)
+    count, heads = dt_ref.shape
+    rows = count * heads
+    inner = heads * HEAD_P
+    groups = heads // HPG
+
+    def head_mask(lanes, per):
+        head = lax.rem(iota((rows, lanes), 0), heads)
+        return head // (HPG if per == groups else 1) == iota((rows, lanes), 1) // (lanes // per)
+
+    @pl.when(j == 0)
+    def _():
+        spread = one_hot(iota((rows, count), 0) // heads == iota((rows, count), 1))
+        dt = mm(spread, dt_ref[...])
+        step = jax.nn.softplus(dt + bias_ref[...])
+        decay = jnp.exp(-step * jnp.exp(log_ref[...]))
+        own = head_mask(heads, heads)
+        step_col = jnp.sum(jnp.where(own, step, 0.0), axis=1, keepdims=True)
+        decay_s[...] = jnp.sum(jnp.where(own, decay, 0.0), axis=1, keepdims=True)
+        xr = mm(spread, x_ref[...].astype(BF16))
+        xr = jnp.where(head_mask(inner, heads), xr, 0.0).astype(BF16)
+        fold = one_hot(lax.rem(iota((inner, HEAD_P), 0), HEAD_P) == iota((inner, HEAD_P), 1))
+        xs[...] = mm(xr, fold).astype(BF16)
+        width = groups * NSTATE
+        gmask = head_mask(width, groups)
+        twice = one_hot(
+            lax.rem(iota((width, 2 * NSTATE), 0), NSTATE)
+            == lax.rem(iota((width, 2 * NSTATE), 1), NSTATE)
+        )
+        ir = jnp.where(gmask, mm(spread, inp_ref[...].astype(BF16)), 0.0).astype(BF16)
+        inp_s[...] = mm(ir, twice) * step_col
+        rr = jnp.where(gmask, mm(spread, rd_ref[...].astype(BF16)), 0.0).astype(BF16)
+        rd_s[...] = mm(rr, twice)
+        acc[...] = jnp.zeros_like(acc)
+
+    lanes = state_ref.shape[1]
+    tiles = lanes // (2 * NSTATE)
+    expand = one_hot(
+        iota((HEAD_P, lanes), 0) == (iota((HEAD_P, lanes), 1) + j * lanes) // NSTATE
+    )
+    collect = one_hot(
+        iota((lanes, HEAD_P), 1) == (iota((lanes, HEAD_P), 0) + j * lanes) // NSTATE
+    )
+    fresh = mm(xs[...], expand) * jnp.concatenate([inp_s[...]] * tiles, axis=1)
+    new = decay_s[...] * state_ref[...] + fresh
+    new_ref[...] = new
+    prod = (new * jnp.concatenate([rd_s[...]] * tiles, axis=1)).astype(BF16)
+    acc[...] += mm(prod, collect)
+
+    @pl.when(j == pl.num_programs(0) - 1)
+    def _():
+        unfold = one_hot(lax.rem(iota((HEAD_P, inner), 1), HEAD_P) == iota((HEAD_P, inner), 0))
+        gatherer = one_hot(iota((count, rows), 1) // heads == iota((count, rows), 0))
+        mask = head_mask(inner, heads)
+        high = acc[...].astype(BF16)
+        low = (acc[...] - high.astype(F32)).astype(BF16)
+        read = jnp.zeros((count, inner), F32)
+        for piece in (high, low):
+            wide = jnp.where(mask, mm(piece, unfold), 0.0).astype(BF16)
+            read = read + mm(gatherer, wide)
+        gated = read * jax.nn.silu(z_ref[...].astype(F32))
+        size = HPG * HEAD_P
+        for g in range(groups):
+            cols = slice(g * size, (g + 1) * size)
+            part = gated[:, cols]
+            part = part * lax.rsqrt(jnp.mean(part * part, axis=-1, keepdims=True) + EPSILON)
+            y_ref[:, cols] = (part * gain_ref[:, cols]).astype(BF16)
+
+
+def state_step(
+    proj_x, proj_z, proj_bc, proj_dt, tail_x, tail_bc, taps_x, taps_bc, ssm_state,
+    dt_bias, decay_log, group_gain,
+):
+    window_x = jnp.concatenate([tail_x, proj_x[:, None]], axis=1).astype(F32)
+    conv_x = jax.nn.silu(jnp.sum(window_x * taps_x.astype(F32)[None], axis=1))
+    window_bc = jnp.concatenate([tail_bc, proj_bc[:, None]], axis=1).astype(F32)
+    conv_bc = jax.nn.silu(jnp.sum(window_bc * taps_bc.astype(F32)[None], axis=1))
+    count, heads, width = ssm_state.shape
+    rows = count * heads
+    full = lambda a: pl.BlockSpec(a.shape, lambda j: (0,) * a.ndim)
+    small = (
+        conv_x, proj_z, conv_bc[:, 0], conv_bc[:, 1], proj_dt,
+        dt_bias[None], decay_log[None], group_gain[None],
+    )
+    block = pl.BlockSpec((rows, LANES), lambda j: (0, j))
+    y_out, new_state = pl.pallas_call(
+        state_kernel,
+        grid=(width // LANES,),
+        in_specs=[full(a) for a in small] + [block],
+        out_specs=[pl.BlockSpec((count, heads * HEAD_P), lambda j: (0, 0)), block],
+        out_shape=[
+            jax.ShapeDtypeStruct((count, heads * HEAD_P), BF16),
+            jax.ShapeDtypeStruct((rows, width), F32),
+        ],
+        scratch_shapes=[
+            pltpu.VMEM((rows, HEAD_P), BF16),
+            pltpu.VMEM((rows, 2 * NSTATE), F32),
+            pltpu.VMEM((rows, 2 * NSTATE), F32),
+            pltpu.VMEM((rows, 1), F32),
+            pltpu.VMEM((rows, HEAD_P), F32),
+        ],
+        name="state_step",
+    )(*small, ssm_state.reshape(rows, width))
+    return y_out, new_state.reshape(count, heads, width)
+
+
+def layer_kernel(
+    y_ref, resid_ref, gain_ref, bgate_ref, gw_ref, ids_ref, ew_ref,
+    oproj_hbm, dg_hbm, du_hbm, dd_hbm, eg_hbm, eu_hbm, ed_hbm,
+    out_ref,
+    oproj, dg, du, dd, eg, eu, ed,
+    ybuf, pbuf, mbuf, nbuf, wide_s, sbuf, dbuf, obuf, rbuf,
+    wsem, ysend, yrecv, msend, mrecv, nsend, nrecv, fsend, dsend, drecv, rsend, rrecv,
+):
+    n, cores = lax.axis_size("ep"), lax.axis_size("tp")
+    me, t = lax.axis_index("ep"), lax.axis_index("tp")
+    other = 1 - t
+    plane = PLANE if n % PLANE == 0 else 1
+    depth = n // plane
+    zz, q = me // plane, lax.rem(me, plane)
+    count, features = resid_ref.shape
+    half = count // cores
+    batch = n * count
+
+    loads = [
+        pltpu.make_async_copy(a, b, wsem.at[i])
+        for i, (a, b) in enumerate(
+            ((oproj_hbm, oproj), (dg_hbm, dg), (du_hbm, du), (eg_hbm, eg),
+             (eu_hbm, eu), (dd_hbm, dd), (ed_hbm, ed))
+        )
+    ]
+    barrier = pltpu.get_barrier_semaphore()
+
+    def greet(k, _):
+        peer = lax.rem(me + k, n)
+        for core in range(cores):
+            pl.semaphore_signal(barrier, inc=1, device_id=(peer, core), device_id_type=MESH)
+        return 0
+
+    lax.fori_loop(1, n, greet, 0)
+    pl.semaphore_signal(barrier, inc=1, device_id=(me, other), device_id_type=MESH)
+    for load in loads:
+        load.start()
+    ybuf[me] = y_ref[...]
+    pl.semaphore_wait(barrier, n * cores - 1)
+
+    def remote(src, dst, send, recv, device):
+        return pltpu.make_async_remote_copy(
+            src_ref=src, dst_ref=dst, send_sem=send, recv_sem=recv,
+            device_id=device, device_id_type=MESH,
+        )
+
+    def beside(k):
+        return zz * plane + lax.rem(q + k, plane)
+
+    def across(k):
+        return lax.rem(zz + k, depth) * plane + q
+
+    def all_gather(first, buf, send, recv, landed):
+        for k in range(1, depth):
+            peer = across(k)
+            remote(first, buf.at[me], send.at[peer], recv.at[me], (peer, t)).start()
+        for k in range(1, plane):
+            peer = beside(k)
+            remote(first, buf.at[me], send.at[peer], recv.at[me], (peer, t)).start()
+        landed(me)
+        for k in range(1, depth):
+            source = across(depth - k)
+            remote(buf.at[source], buf.at[source], send.at[source], recv.at[source], (me, other)).wait_recv()
+            for i in range(1, plane):
+                peer = beside(i)
+                slot = (source // plane) * plane + lax.rem(peer, plane)
+                remote(buf.at[source], buf.at[source], send.at[slot], recv.at[source], (peer, t)).start()
+            landed(source)
+
+        def arrive(level, _):
+            base = lax.rem(zz + level, depth) * plane
+            for i in range(1, plane):
+                source = base + lax.rem(q + i, plane)
+                remote(buf.at[source], buf.at[source], send.at[source], recv.at[source], (me, other)).wait_recv()
+                landed(source)
+            return 0
+
+        lax.fori_loop(0, depth, arrive, 0)
+
+    def drain(first, send):
+        def one(k, _):
+            peer = lax.rem(me + k, n)
+            remote(first, first, send.at[peer], send.at[peer], (me, other)).wait_send()
+            return 0
+
+        lax.fori_loop(1, n, one, 0)
+
+    all_gather(y_ref, ybuf, ysend, yrecv, lambda source: None)
+    loads[0].wait()
+    partial = mm(ybuf[...].reshape(batch, ybuf.shape[2]), oproj[...])
+    pbuf[...] = partial.astype(BF16).reshape(pbuf.shape)
+    mbuf[t, me] = pbuf[me]
+
+    def scatter(k, _):
+        peer = lax.rem(me + k, n)
+        for core in range(cores):
+            remote(pbuf.at[peer], mbuf.at[t, me], msend.at[core, peer], mrecv.at[t, me], (peer, core)).start()
+        return 0
+
+    lax.fori_loop(1, n, scatter, 0)
+    remote(pbuf.at[me], mbuf.at[t, me], msend.at[other, me], mrecv.at[t, me], (me, other)).start()
+
+    def collect(k, _):
+        peer = lax.rem(me + k, n)
+        for core in range(cores):
+            remote(pbuf.at[peer], mbuf.at[core, peer], msend.at[core, peer], mrecv.at[core, peer], (me, other)).wait_recv()
+        return 0
+
+    lax.fori_loop(1, n, collect, 0)
+    remote(pbuf.at[me], mbuf.at[other, me], msend.at[other, me], mrecv.at[other, me], (me, other)).wait_recv()
+
+    mixed = jnp.concatenate(
+        [sum(mbuf[core, e].astype(F32) for core in range(cores)) for e in range(n)], axis=1
+    )
+    widened = (resid_ref[...].astype(F32) + mixed).astype(BF16).astype(F32)
+    wide_s[...] = widened
+    normed = (
+        widened
+        * lax.rsqrt(jnp.mean(widened * widened, axis=-1, keepdims=True) + EPSILON)
+        * gain_ref[...]
+    ).astype(BF16)
+    part = features // cores
+    for core in range(cores):
+        nbuf[core, me] = normed[:, core * part : (core + 1) * part]
+
+    def pass_on(source):
+        @pl.when(source != me)
+        def _():
+            remote(nbuf.at[t, source], nbuf.at[t, source], fsend.at[source], nrecv.at[t, source], (me, other)).start()
+
+    all_gather(nbuf.at[t, me], nbuf.at[t], nsend, nrecv.at[t], pass_on)
+
+    def passed(k, _):
+        peer = lax.rem(me + k, n)
+        remote(nbuf.at[other, peer], nbuf.at[other, peer], fsend.at[peer], nrecv.at[other, peer], (me, other)).wait_recv()
+        return 0
+
+    lax.fori_loop(1, n, passed, 0)
+
+    chunks = [nbuf[core].reshape(batch, part) for core in range(cores)]
+    for load in loads[1:5]:
+        load.wait()
+
+    def project(w):
+        return sum(mm(chunks[core], w[core * part : (core + 1) * part, :]) for core in range(cores))
+
+    score = sum(
+        jnp.sum(
+            chunks[core].astype(F32) * bgate_ref[:, core * part : (core + 1) * part].astype(F32),
+            axis=1, keepdims=True,
+        )
+        for core in range(cores)
+    )
+    dense_hidden = (jax.nn.sigmoid(score) * jax.nn.silu(project(dg)) * project(du)).astype(BF16)
+    pick = (iota(gw_ref.shape, 1) == me // (n // GROUPS)).astype(F32)
+    coarse = jnp.sum(gw_ref[...] * pick, axis=1, keepdims=True)
+    mine = (ids_ref[...] == me).astype(F32)
+    weight = jnp.sum(mine * (ew_ref[...] * coarse), axis=1, keepdims=True)
+    row_hidden = (weight * jax.nn.silu(project(eg.at[0])) * project(eu.at[0])).astype(BF16)
+    for load in loads[5:]:
+        load.wait()
+    step = 512
+    for start in range(0, features, step):
+        cols = slice(start, start + step)
+        block = mm(dense_hidden, dd[:, cols]) + mm(row_hidden, ed[0, :, cols])
+        block = block.reshape(n, cores, half, step)
+        for core in range(cores):
+            sbuf[core, :, :, cols] = block[:, core].astype(BF16)
+
+    def swap(level):
+        base = pl.ds(lax.rem(zz + 1 + level, depth) * plane, plane)
+        return remote(sbuf.at[other, base], dbuf.at[base], dsend.at[level], drecv.at[level], (me, other))
+
+    for level in range(depth):
+        swap(level).start()
+    for level in range(depth):
+        swap(level).wait_recv()
+        base = lax.rem(zz + 1 + level, depth) * plane
+        for i in range(plane):
+            dest = base + i
+            total = sbuf[t, dest].astype(F32) + dbuf[dest].astype(F32)
+            obuf[dest] = total.astype(BF16)
+            if level < depth - 1:
+                remote(obuf.at[dest], rbuf.at[me], rsend.at[dest], rrecv.at[me], (dest, t)).start()
+            else:
+                @pl.when(dest != me)
+                def _():
+                    remote(obuf.at[dest], rbuf.at[me], rsend.at[dest], rrecv.at[me], (dest, t)).start()
+
+    total = wide_s[pl.ds(pl.multiple_of(t * half, half), half), :]
+    total = total + sbuf[t, me].astype(F32) + dbuf[me].astype(F32)
+
+    def final(k, total):
+        peer = lax.rem(me + k, n)
+        remote(obuf.at[peer], rbuf.at[peer], rsend.at[peer], rrecv.at[peer], (me, other)).wait_recv()
+        return total + rbuf[peer].astype(F32)
+
+    total = lax.fori_loop(1, n, final, total)
+    out_ref[...] = total.astype(BF16)
+    drain(y_ref, ysend)
+    drain(nbuf.at[t, me], nsend)
+    drain(nbuf.at[t, me], fsend)
+    drain(obuf.at[me], rsend)
+    for core in range(cores):
+        drain(pbuf.at[me], msend.at[core])
+    remote(pbuf.at[me], mbuf.at[t, me], msend.at[other, me], mrecv.at[t, me], (me, other)).wait_send()
+    for level in range(depth):
+        swap(level).wait_send()
+
+
+def layer(
+    y_out, resid, out_proj, ffn_gain, dense_gate, dense_up, dense_down, branch_gate,
+    group_weights, expert_ids, expert_weights, exp_gate, exp_up, exp_down,
+):
+    n, cores = lax.axis_size("ep"), lax.axis_size("tp")
+    count, features = resid.shape
+    half = count // cores
+    depth = n // PLANE if n % PLANE == 0 else n
+    vmem = pl.BlockSpec(memory_space=pltpu.VMEM)
+    hbm = pl.BlockSpec(memory_space=pl.ANY)
+    weights = (out_proj, dense_gate, dense_up, dense_down, exp_gate, exp_up, exp_down)
+    dma = pltpu.SemaphoreType.DMA
+    return pl.pallas_call(
+        layer_kernel,
+        in_specs=[vmem] * 7 + [hbm] * 7,
+        out_specs=vmem,
+        out_shape=jax.ShapeDtypeStruct((half, features), BF16),
+        scratch_shapes=[pltpu.VMEM(w.shape, w.dtype) for w in weights]
+        + [
+            pltpu.VMEM((n,) + y_out.shape, BF16),
+            pltpu.VMEM((n, count, out_proj.shape[1]), BF16),
+            pltpu.VMEM((cores, n, count, out_proj.shape[1]), BF16),
+            pltpu.VMEM((cores, n, count, features // cores), BF16),
+            pltpu.VMEM((count, features), F32),
+            pltpu.VMEM((cores, n, half, features), BF16),
+            pltpu.VMEM((n, half, features), BF16),
+            pltpu.VMEM((n, half, features), BF16),
+            pltpu.VMEM((n, half, features), BF16),
+            dma((7,)), dma((n,)), dma((n,)), dma((cores, n)), dma((cores, n)),
+            dma((n,)), dma((cores, n)), dma((n,)), dma((depth,)), dma((depth,)),
+            dma((n,)), dma((n,)),
+        ],
+        compiler_params=pltpu.CompilerParams(
+            collective_id=0, has_side_effects=True, vmem_limit_bytes=60 * 1024 * 1024
+        ),
+        name="layer_step",
+    )(
+        y_out, resid, ffn_gain[None], branch_gate[None], group_weights, expert_ids,
+        expert_weights, *weights,
+    )
 
 
 def state_update(
@@ -77,6 +460,16 @@
     exp_up,
     exp_down,
 ):
+    if out_proj.shape[1] % 128 == 0 and lax.axis_size("tp") == 2:
+        y_out, new_state = state_step(
+            proj_x, proj_z, proj_bc, proj_dt, tail_x, tail_bc, taps_x, taps_bc, ssm_state,
+            dt_bias, decay_log, group_gain,
+        )
+        out = layer(
+            y_out, resid, out_proj, ffn_gain, dense_gate, dense_up, dense_down, branch_gate,
+            group_weights, expert_ids, expert_weights, exp_gate, exp_up, exp_down,
+        )
+        return (out, new_state)
     y_out, new_state = state_update(
         proj_x,
         proj_z,

time: 272 us -> 70.2 us (0.26)
  the two profiles are of different devices: /device:TPU:0 before, /device:TPU:12 now
where the time goes in v1:
time: 70.2 us; the launch traced here: 69.6 us
  Pallas kernels  60 us (85%)
  local copies, waits for them, and re-layouts  5 us (7%)
  other arithmetic  3.96 us (6%)
    pallas_call x1, Pallas kernels, layer(): pl.pallas_call(layer_kernel, in_specs=[vmem] * 7 + [hbm] * 7, out_specs=v...  50.4 us
    pallas_call x1, Pallas kernels, state_step(): pl.pallas_call(state_kernel, grid=(width // LANES,), in_specs=[full(a) fo...  9.56 us
    unnamed x12, local copies, waits for them, and re-layouts  3.78 us

profile of v1, /device:TPU:12, one launch (start us, length us, event | category | flops | bytes accessed | tf_op | source)
XLA Modules:
  0.0 69.6 jit_solution(12392306059338629218)
XLA Ops:
  0.6 0.0 copy-start.2
  0.6 0.0 copy-start
  0.7 0.0 copy-start.1
  0.7 0.0 copy-start.3
  0.7 0.7 %convert_element_type.15 = f32[4,2,256]{2,1,0:T(2,128)S(1)} convert(bf16[4,2,256]{2,1,0:T(2,128)(2,1)} %param.33) | non-fusion elementwise | flops 2048 | bytes 12288 | tf_op jit(solution)/shard_map/convert_element_type | solution.py:117
  1.4 0.9 %multiply_reduce_fusion.1 = f32[16,2,256]{2,1,0:T(2,128)S(1)} fusion(bf16[16,1,2,256]{3,2,1,0:T(2,128)(2,1)} %bitcast.14, bf16[16,3,2,256]{3,2,1,0:T(2,128)(2,1)} %param.31, f32[4,2,256]{2,1,0:T(2,128)S(1)} %convert_element_type.15), kind=kLoop, calls=%fused_computation.1 | loop fusion | flops 122880 | bytes 106496 | tf_op jit(solution)/shard_map/reduce_sum | solution.py:117
  2.3 0.6 slice_bitcast_fusion
  3.0 0.7 %convert_element_type.13 = f32[4,1024]{1,0:T(4,128)S(1)} convert(bf16[4,1024]{1,0:T(4,128)(2,1)} %param.32) | non-fusion elementwise | flops 4096 | bytes 24576 | tf_op jit(solution)/shard_map/convert_element_type | solution.py:115
  3.7 0.9 %multiply_reduce_fusion = f32[16,1024]{1,0:T(8,128)S(1)} fusion(bf16[16,1,1024]{2,0,1:T(8,128)(2,1)} %bitcast.13, bf16[16,3,1024]{2,0,1:T(8,128)(2,1)} %param.30, f32[4,1024]{1,0:T(4,128)S(1)} %convert_element_type.13), kind=kLoop, calls=%fused_computation | loop fusion | flops 245760 | bytes 212992 | tf_op jit(solution)/shard_map/reduce_sum | solution.py:115
  4.6 0.6 divide_multiply_fusion.x_ref
  5.3 9.6 %state_step.1 = (bf16[16,1024]{1,0:T(8,128)(2,1)}, f32[256,4096]{1,0:T(8,128)}) custom-call(f32[16,1024]{1,0:T(8,128)} %divide_multiply_fusion.x_ref, bf16[16,1024]{1,0:T(8,128)(2,1)} %z_ref.1, f32[16,256]{1,0:T(8,128)} %get-tuple-element.7.inp_ref, f32[16,256]{1,0:T(8,128)} %get-tuple-element.6.rd_ref, bf16[16,16]{1,0:T(8,128)(2,1)} %dt_ref.1, ...), custom_call_target="tpu_custom_call" | custom-call | tf_op jit(solution)/shard_map/state_step/pallas_call | solution.py:126
  14.8 0.0 copy-done.2
  14.8 0.8 %copy.32.gw_ref = f32[256,4]{1,0:T(8,128)} copy(f32[256,4]{0,1:T(4,128)S(1)} %copy-done.2) | data formatting | bytes 8192 | tf_op args[19]
  15.6 0.0 copy-done
  15.6 0.8 %copy.33.ids_ref = s32[256,6]{1,0:T(8,128)} copy(s32[256,6]{0,1:T(8,128)S(1)} %copy-done) | data formatting | bytes 12288 | tf_op args[20]
  16.4 0.0 copy-done.1
  16.4 0.8 %copy.34.ew_ref = f32[256,6]{1,0:T(8,128)} copy(f32[256,6]{0,1:T(8,128)S(1)} %copy-done.1) | data formatting | bytes 12288 | tf_op args[21]
  17.2 0.0 copy-done.3
  17.2 0.6 broadcast_in_dim.29.bgate_ref
  17.8 50.4 %layer_step.1 = bf16[8,2048]{1,0:T(8,128)(2,1)} custom-call(bf16[16,1024]{1,0:T(8,128)(2,1)} %get-tuple-element.4.y_ref, bf16[16,2048]{1,0:T(8,128)(2,1)} %resid_ref.1, f32[1,2048]{1,0:T(1,128)} %bitcast.15, bf16[1,2048]{1,0:T(2,128)(2,1)} %broadcast_in_dim.29.bgate_ref, f32[256,4]{1,0:T(8,128)} %copy.32.gw_ref, s32[256,6]{1,0:T(8,128)} %copy.33.ids_ref, ...), custom_call_target="tpu_custom_call" | custom-call | tf_op jit(solution)/shard_map/layer_step/pallas_call | solution.py:369
  68.3 1.4 %copy.37 = bf16[8,2048]{1,0:T(8,128)(2,1)} copy(bf16[8,2048]{1,0:T(8,128)(2,1)} %layer_step.1) | data formatting | bytes 65536
  (1 shorter events, 0.0 us)
Async XLA Ops:
  0.6 14.2 %copy-start.2 = (f32[256,4]{0,1:T(4,128)S(1)}, f32[256,4]{0,1:T(4,128)}, u32[]{:S(2)}) copy-start(f32[256,4]{0,1:T(4,128)} %param.44) | copy-start | bytes 12292
  0.6 15.0 %copy-start = (s32[256,6]{0,1:T(8,128)S(1)}, s32[256,6]{0,1:T(8,128)}, u32[]{:S(2)}) copy-start(s32[256,6]{0,1:T(8,128)} %param.45) | copy-start | bytes 18436
  0.7 15.8 %copy-start.1 = (f32[256,6]{0,1:T(8,128)S(1)}, f32[256,6]{0,1:T(8,128)}, u32[]{:S(2)}) copy-start(f32[256,6]{0,1:T(8,128)} %param.46) | copy-start | bytes 18436
  0.7 16.6 %copy-start.3 = (bf16[2048]{0:T(1024)(128)(2,1)S(1)}, bf16[2048]{0:T(1024)(128)(2,1)}, u32[]{:S(2)}) copy-start(bf16[2048]{0:T(1024)(128)(2,1)} %param.43) | copy-start | bytes 12292

commit v2 on v1

--- a/solution.py
+++ b/solution.py
@@ -35,7 +35,7 @@
 
 
 def state_kernel(
-    x_ref, z_ref, inp_ref, rd_ref, dt_ref, bias_ref, log_ref, gain_ref, state_ref,
+    x_ref, z_ref, bc_ref, tail_x_ref, tail_bc_ref, taps_x_ref, taps_bc_ref, dt_ref, bias_ref, log_ref, gain_ref, state_ref,
     y_ref, new_ref, xs, inp_s, rd_s, decay_s, acc,
 ):
     j = pl.program_id(0)
@@ -51,13 +51,25 @@
     @pl.when(j == 0)
     def _():
         spread = one_hot(iota((rows, count), 0) // heads == iota((rows, count), 1))
+        taps = taps_x_ref.shape[0]
+        taps_x = taps_x_ref[...].astype(F32)
+        conv_x = x_ref[...].astype(F32) * taps_x[taps - 1 : taps]
+        for w in range(taps - 1):
+            conv_x = conv_x + tail_x_ref[w].astype(F32) * taps_x[w : w + 1]
+        conv_x = jax.nn.silu(conv_x)
+        conv_bc = []
+        for i in range(2):
+            conv = bc_ref[:, i, :].astype(F32) * taps_bc_ref[taps - 1, i : i + 1, :].astype(F32)
+            for w in range(taps - 1):
+                conv = conv + tail_bc_ref[:, w, i, :].astype(F32) * taps_bc_ref[w, i : i + 1, :].astype(F32)
+            conv_bc.append(jax.nn.silu(conv))
         dt = mm(spread, dt_ref[...])
         step = jax.nn.softplus(dt + bias_ref[...])
         decay = jnp.exp(-step * jnp.exp(log_ref[...]))
         own = head_mask(heads, heads)
         step_col = jnp.sum(jnp.where(own, step, 0.0), axis=1, keepdims=True)
         decay_s[...] = jnp.sum(jnp.where(own, decay, 0.0), axis=1, keepdims=True)
-        xr = mm(spread, x_ref[...].astype(BF16))
+        xr = mm(spread, conv_x.astype(BF16))
         xr = jnp.where(head_mask(inner, heads), xr, 0.0).astype(BF16)
         fold = one_hot(lax.rem(iota((inner, HEAD_P), 0), HEAD_P) == iota((inner, HEAD_P), 1))
         xs[...] = mm(xr, fold).astype(BF16)
@@ -67,9 +79,9 @@
             lax.rem(iota((width, 2 * NSTATE), 0), NSTATE)
             == lax.rem(iota((width, 2 * NSTATE), 1), NSTATE)
         )
-        ir = jnp.where(gmask, mm(spread, inp_ref[...].astype(BF16)), 0.0).astype(BF16)
+        ir = jnp.where(gmask, mm(spread, conv_bc[0].astype(BF16)), 0.0).astype(BF16)
         inp_s[...] = mm(ir, twice) * step_col
-        rr = jnp.where(gmask, mm(spread, rd_ref[...].astype(BF16)), 0.0).astype(BF16)
+        rr = jnp.where(gmask, mm(spread, conv_bc[1].astype(BF16)), 0.0).astype(BF16)
         rd_s[...] = mm(rr, twice)
         acc[...] = jnp.zeros_like(acc)
 
@@ -111,15 +123,11 @@
     proj_x, proj_z, proj_bc, proj_dt, tail_x, tail_bc, taps_x, taps_bc, ssm_state,
     dt_bias, decay_log, group_gain,
 ):
-    window_x = jnp.concatenate([tail_x, proj_x[:, None]], axis=1).astype(F32)
-    conv_x = jax.nn.silu(jnp.sum(window_x * taps_x.astype(F32)[None], axis=1))
-    window_bc = jnp.concatenate([tail_bc, proj_bc[:, None]], axis=1).astype(F32)
-    conv_bc = jax.nn.silu(jnp.sum(window_bc * taps_bc.astype(F32)[None], axis=1))
     count, heads, width = ssm_state.shape
     rows = count * heads
     full = lambda a: pl.BlockSpec(a.shape, lambda j: (0,) * a.ndim)
     small = (
-        conv_x, proj_z, conv_bc[:, 0], conv_bc[:, 1], proj_dt,
+        proj_x, proj_z, proj_bc, tail_x.transpose(1, 0, 2), tail_bc, taps_x, taps_bc, proj_dt,
         dt_bias[None], decay_log[None], group_gain[None],
     )
     block = pl.BlockSpec((rows, LANES), lambda j: (0, j))
@@ -149,8 +157,8 @@
     oproj_hbm, dg_hbm, du_hbm, dd_hbm, eg_hbm, eu_hbm, ed_hbm,
     out_ref,
     oproj, dg, du, dd, eg, eu, ed,
-    ybuf, pbuf, mbuf, nbuf, wide_s, sbuf, dbuf, obuf, rbuf,
-    wsem, ysend, yrecv, msend, mrecv, nsend, nrecv, fsend, dsend, drecv, rsend, rrecv,
+    ybuf, pbuf, mbuf, nbuf, wide_s, sbuf, dbuf, obuf, rbuf, zbuf, hbuf,
+    wsem, ysend, yrecv, msend, mrecv, nsend, nrecv, fsend, dsend, drecv, rsend, rrecv, zsend, zrecv,
 ):
     n, cores = lax.axis_size("ep"), lax.axis_size("tp")
     me, t = lax.axis_index("ep"), lax.axis_index("tp")
@@ -290,18 +298,22 @@
     def project(w):
         return sum(mm(chunks[core], w[core * part : (core + 1) * part, :]) for core in range(cores))
 
+    bgate = bgate_ref[...].astype(F32)
+    bgate = jnp.concatenate([bgate[i : i + 1] for i in range(bgate.shape[0])], axis=1)
     score = sum(
         jnp.sum(
-            chunks[core].astype(F32) * bgate_ref[:, core * part : (core + 1) * part].astype(F32),
+            chunks[core].astype(F32) * bgate[:, core * part : (core + 1) * part],
             axis=1, keepdims=True,
         )
         for core in range(cores)
     )
     dense_hidden = (jax.nn.sigmoid(score) * jax.nn.silu(project(dg)) * project(du)).astype(BF16)
-    pick = (iota(gw_ref.shape, 1) == me // (n // GROUPS)).astype(F32)
-    coarse = jnp.sum(gw_ref[...] * pick, axis=1, keepdims=True)
+    pick = (iota(gw_ref.shape, 0) == me // (n // GROUPS)).astype(F32)
+    coarse = jnp.sum(gw_ref[...] * pick, axis=0, keepdims=True)
     mine = (ids_ref[...] == me).astype(F32)
-    weight = jnp.sum(mine * (ew_ref[...] * coarse), axis=1, keepdims=True)
+    weight_row = jnp.sum(mine * (ew_ref[...] * coarse), axis=0, keepdims=True)
+    diagonal = iota((batch, batch), 0) == iota((batch, batch), 1)
+    weight = jnp.sum(jnp.where(diagonal, weight_row, 0.0), axis=1, keepdims=True)
     row_hidden = (weight * jax.nn.silu(project(eg.at[0])) * project(eu.at[0])).astype(BF16)
     for load in loads[5:]:
         load.wait()
@@ -319,39 +331,63 @@
 
     for level in range(depth):
         swap(level).start()
+    def in_plane(level, i):
+        base = lax.rem(zz + 1 + level, depth) * plane
+        peer = lax.rem(q + i, plane)
+        return remote(
+            obuf.at[base + peer], rbuf.at[base + q], rsend.at[base + peer], rrecv.at[base + q],
+            (zz * plane + peer, t),
+        )
+
+    def summed(dest):
+        return sbuf[t, dest].astype(F32) + dbuf[dest].astype(F32)
+
+    def to_owner(level):
+        owner = lax.rem(zz + 1 + level, depth)
+        return remote(
+            zbuf.at[owner], hbuf.at[zz], zsend.at[owner], zrecv.at[zz], (owner * plane + q, t)
+        )
+
+    def finish(level):
+        owner = lax.rem(zz + 1 + level, depth)
+        base = owner * plane
+        total = summed(base + q)
+        for i in range(1, plane):
+            source = base + lax.rem(q + i, plane)
+            remote(rbuf.at[source], rbuf.at[source], rsend.at[source], rrecv.at[source], (me, other)).wait_recv()
+            total = total + rbuf[source].astype(F32)
+        if level < depth - 1:
+            zbuf[owner] = total.astype(BF16)
+            to_owner(level).start()
+        return total
+
     for level in range(depth):
         swap(level).wait_recv()
         base = lax.rem(zz + 1 + level, depth) * plane
-        for i in range(plane):
-            dest = base + i
-            total = sbuf[t, dest].astype(F32) + dbuf[dest].astype(F32)
-            obuf[dest] = total.astype(BF16)
-            if level < depth - 1:
-                remote(obuf.at[dest], rbuf.at[me], rsend.at[dest], rrecv.at[me], (dest, t)).start()
-            else:
-                @pl.when(dest != me)
-                def _():
-                    remote(obuf.at[dest], rbuf.at[me], rsend.at[dest], rrecv.at[me], (dest, t)).start()
-
-    total = wide_s[pl.ds(pl.multiple_of(t * half, half), half), :]
-    total = total + sbuf[t, me].astype(F32) + dbuf[me].astype(F32)
-
-    def final(k, total):
-        peer = lax.rem(me + k, n)
-        remote(obuf.at[peer], rbuf.at[peer], rsend.at[peer], rrecv.at[peer], (me, other)).wait_recv()
-        return total + rbuf[peer].astype(F32)
-
-    total = lax.fori_loop(1, n, final, total)
+        for i in range(1, plane):
+            dest = base + lax.rem(q + i, plane)
+            obuf[dest] = summed(dest).astype(BF16)
+            in_plane(level, i).start()
+        if level > 0:
+            finish(level - 1)
+    total = finish(depth - 1) + wide_s[pl.ds(pl.multiple_of(t * half, half), half), :]
+    for k in range(1, depth):
+        source = lax.rem(zz + depth - k, depth)
+        remote(hbuf.at[source], hbuf.at[source], zsend.at[source], zrecv.at[source], (me, other)).wait_recv()
+        total = total + hbuf[source].astype(F32)
     out_ref[...] = total.astype(BF16)
     drain(y_ref, ysend)
     drain(nbuf.at[t, me], nsend)
     drain(nbuf.at[t, me], fsend)
-    drain(obuf.at[me], rsend)
     for core in range(cores):
         drain(pbuf.at[me], msend.at[core])
     remote(pbuf.at[me], mbuf.at[t, me], msend.at[other, me], mrecv.at[t, me], (me, other)).wait_send()
     for level in range(depth):
         swap(level).wait_send()
+        for i in range(1, plane):
+            in_plane(level, i).wait_send()
+        if level < depth - 1:
+            to_owner(level).wait_send()
 
 
 def layer(
@@ -382,17 +418,19 @@
             pltpu.VMEM((n, half, features), BF16),
             pltpu.VMEM((n, half, features), BF16),
             pltpu.VMEM((n, half, features), BF16),
+            pltpu.VMEM((depth, half, features), BF16),
+            pltpu.VMEM((depth, half, features), BF16),
             dma((7,)), dma((n,)), dma((n,)), dma((cores, n)), dma((cores, n)),
             dma((n,)), dma((cores, n)), dma((n,)), dma((depth,)), dma((depth,)),
-            dma((n,)), dma((n,)),
+            dma((n,)), dma((n,)), dma((depth,)), dma((depth,)),
         ],
         compiler_params=pltpu.CompilerParams(
             collective_id=0, has_side_effects=True, vmem_limit_bytes=60 * 1024 * 1024
         ),
         name="layer_step",
     )(
-        y_out, resid, ffn_gain[None], branch_gate[None], group_weights, expert_ids,
-        expert_weights, *weights,
+        y_out, resid, ffn_gain[None], branch_gate.reshape(-1, 128), group_weights.T, expert_ids.T,
+        expert_weights.T, *weights,
     )
 
 

time: 70.2 us -> 61.1 us (0.87)
  the two profiles are of different devices: /device:TPU:12 before, /device:TPU:0 now
where the time goes in v2:
time: 61.1 us; the launch traced here: 60.7 us
  Pallas kernels  58.7 us (96%)
  local copies, waits for them, and re-layouts  1.38 us (2%)
  between operations  0.64 us (1%)
    pallas_call x1, Pallas kernels, layer(): pl.pallas_call(layer_kernel, in_specs=[vmem] * 7 + [hbm] * 7, out_specs=v...  49 us
    pallas_call x1, Pallas kernels, state_step(): pl.pallas_call(state_kernel, grid=(width // LANES,), in_specs=[full(a) fo...  9.71 us
    unnamed x1, local copies, waits for them, and re-layouts  1.38 us

profile of v2, /device:TPU:0, one launch (start us, length us, event | category | flops | bytes accessed | tf_op | source)
XLA Modules:
  0.0 60.7 jit_solution(11387583433306001431)
XLA Ops:
  0.6 9.7 %state_step.1 = (bf16[16,1024]{1,0:T(8,128)(2,1)}, f32[256,4096]{1,0:T(8,128)}) custom-call(bf16[16,1024]{1,0:T(8,128)(2,1)} %x_ref.1, bf16[16,1024]{1,0:T(8,128)(2,1)} %z_ref.1, bf16[16,2,256]{2,1,0:T(2,128)(2,1)} %bc_ref.1, bf16[3,16,1024]{2,1,0:T(8,128)(2,1)} %bitcast.12, bf16[16,3,2,256]{3,2,1,0:T(2,128)(2,1)} %tail_bc_ref.1, ...), custom_call_target="tpu_custom_call" | custom-call | tf_op jit(solution)/shard_map/state_step/pallas_call | solution.py:134
  10.3 49.0 %layer_step.1 = bf16[8,2048]{1,0:T(8,128)(2,1)} custom-call(bf16[16,1024]{1,0:T(8,128)(2,1)} %get-tuple-element.4.y_ref, bf16[16,2048]{1,0:T(8,128)(2,1)} %resid_ref.1, f32[1,2048]{1,0:T(1,128)} %bitcast.13, bf16[16,128]{1,0:T(8,128)(2,1)} %bitcast.16, f32[4,256]{1,0:T(4,128)} %bitcast.17, s32[6,256]{1,0:T(8,128)} %bitcast.14, f32[6,256]{1,0:T(8,128)} %bitcast.15, ...), custom_call_target="tpu_custom_call" | custom-call | tf_op jit(solution)/shard_map/layer_step/pallas_call | solution.py:405
  59.3 1.4 %copy.28 = bf16[8,2048]{1,0:T(8,128)(2,1)} copy(bf16[8,2048]{1,0:T(8,128)(2,1)} %layer_step.1) | data formatting | bytes 65536
